TPU v7x, 32 devices: a whole 2x2x4 slice. The times are simulated.
32 devices in a mesh: fs: 8 (over z, y), tp: 4 (over x, core).
Axes of the slice: x: 2, y: 2, z: 4, core: 2. Of those that a mesh axis runs over, the one named last changes fastest.
Arguments:
- inputs: bfloat16 [4096, 2112], P('fs', 'tp'), may hold values from -6 to 6
- w_conv_up: bfloat16 [2112, 2816], P('fs', 'tp'), may hold values from -0.125 to 0.125
- w_gate_up: bfloat16 [2112, 2816], P('fs', 'tp'), may hold values from -0.125 to 0.125
- w_down: bfloat16 [2816, 2112], P('tp', 'fs'), may hold values from -0.109375 to 0.109375
- taps: float32 [3, 2816], replicated, may hold values from -3 to 3
- conv_bias: float32 [2816], replicated, may hold values from -3 to 3
- cotangent: bfloat16 [4096, 2112], P('fs', 'tp'), may hold values from -6 to 6
Outputs:
- grad_inputs: bfloat16 [4096, 2112], P('fs', 'tp')
- grad_conv_up: float32 [2112, 2816], P('fs', 'tp')
- unit_norms: float32 [2816], P('tp')
- grad_taps: float32 [3, 2816], replicated
- grad_bias: float32 [2816], replicated
All inputs are finite; a program needn't handle non-finite values.
Results may differ from a plain program's by a relative error of at most 0.018.
Values may be sent and summed in bfloat16 or wider, within the bound.
A program may use at most 64 MiB of HBM per device.

v0:
```python
import math
import jax
import jax.numpy as jnp
from jax import lax
from jax.sharding import PartitionSpec as P

TAPS = 3


def shifted(block, axis, distance):
    devices = range(lax.axis_size(axis))
    route = [(i - distance, i) for i in devices if i - distance in devices]
    return lax.ppermute(block, axis, route)


def gelu_parts(value):
    normal_cdf = 0.5 * (1.0 + jax.scipy.special.erf(value / math.sqrt(2.0)))
    density = jnp.exp(-0.5 * value * value) / math.sqrt(2.0 * math.pi)
    return (value * normal_cdf, normal_cdf + value * density)


def per_device(inputs, w_conv_up, w_gate_up, w_down, taps, conv_bias, cotangent):
    span = TAPS - 1
    rows = inputs.shape[0]
    width = w_conv_up.shape[1]
    col_start = lax.axis_index("tp") * width
    taps_own = lax.dynamic_slice_in_dim(taps, col_start, width, 1)
    bias_own = lax.dynamic_slice_in_dim(conv_bias, col_start, width, 0)
    features, cot_full = (
        lax.all_gather(inputs, "tp", axis=1, tiled=True),
        lax.all_gather(cotangent, "tp", axis=1, tiled=True),
    )
    conv_weight, gate_weight = (
        lax.all_gather(w_conv_up, "fs", axis=0, tiled=True),
        lax.all_gather(w_gate_up, "fs", axis=0, tiled=True),
    )
    columns = cot_full
    d_hidden = lax.dot_general(
        columns,
        lax.all_gather(w_down, "fs", axis=1, tiled=True),
        (((1,), (1,)), ((), ())),
        preferred_element_type=jnp.float32,
    ).astype(jnp.bfloat16)
    up_a = jnp.dot(features, conv_weight, preferred_element_type=jnp.float32).astype(jnp.bfloat16)
    up_b = jnp.dot(features, gate_weight, preferred_element_type=jnp.float32).astype(jnp.bfloat16)
    earlier = shifted(up_a[rows - span :], "fs", 1)
    extended = jnp.concatenate([earlier, up_a], 0).astype(jnp.float32)
    conv_out = bias_own[None, :] + sum(
        (taps_own[i][None, :] * extended[i : i + rows] for i in range(TAPS))
    )
    gelu_value, gelu_slope = gelu_parts(conv_out)
    hidden_grad = d_hidden.astype(jnp.float32)
    d_conv = hidden_grad * up_b.astype(jnp.float32) * gelu_slope
    d_up_b = (hidden_grad * gelu_value).astype(jnp.bfloat16)
    later = shifted(d_conv[:span], "fs", -1)
    d_extended = jnp.concatenate([d_conv, later], 0)
    d_up_a = sum(
        (taps_own[i][None, :] * d_extended[span - i : span - i + rows] for i in range(TAPS))
    ).astype(jnp.bfloat16)
    tap_terms = [jnp.sum(d_conv * extended[i : i + rows], axis=0) for i in range(TAPS)]
    column_part = jnp.stack(tap_terms + [jnp.sum(d_conv, axis=0)], 0)
    contract = (((1,), (1,)), ((), ()))
    partial_sum = lax.dot_general(d_up_a, conv_weight, contract, preferred_element_type=jnp.float32)
    partial_sum = partial_sum + lax.dot_general(
        d_up_b, gate_weight, contract, preferred_element_type=jnp.float32
    )
    grad_inputs = lax.psum_scatter(
        partial_sum.astype(jnp.bfloat16), "tp", scatter_dimension=1, tiled=True
    )
    columns = features
    grad_conv_up = lax.psum_scatter(
        lax.dot_general(
            columns, d_up_a, (((0,), (0,)), ((), ())), preferred_element_type=jnp.float32
        ),
        "fs",
        scatter_dimension=0,
        tiled=True,
    )
    squares = jnp.sum(grad_conv_up * grad_conv_up, axis=0)
    placed = jnp.zeros((TAPS + 1, width * lax.axis_size("tp")), jnp.float32)
    placed = lax.dynamic_update_slice_in_dim(placed, column_part, col_start, 1)
    full_columns = lax.psum(placed, ("fs", "tp"))
    unit_norms = lax.psum(squares, "fs")
    return (grad_inputs, grad_conv_up, unit_norms, full_columns[:TAPS], full_columns[TAPS])


def solution(mesh):
    return jax.shard_map(
        per_device,
        mesh=mesh,
        in_specs=(
            P("fs", "tp"),
            P("fs", "tp"),
            P("fs", "tp"),
            P("tp", "fs"),
            P(),
            P(),
            P("fs", "tp"),
        ),
        out_specs=(P("fs", "tp"), P("fs", "tp"), P("tp"), P(), P()),
        check_vma=False,
    )
```

profile of v0, /device:TPU:0, one launch (start us, length us, event | category | flops | bytes accessed | tf_op | source)
XLA Modules:
  0.0 441.5 jit_solution(5598248172429005860)
XLA Ops:
  10.6 0.8 dynamic_slice.7
  11.4 0.9 dynamic-slice_reduce_fusion.2
  12.3 22.9 %all-gather.10.cloned.1.call-done = bf16[512,2112]{0,1:T(8,128)(2,1)} async-done(((bf16[512,528]{0,1:T(8,128)(2,1)}), bf16[512,2112]{0,1:T(8,128)(2,1)}) %all-gather.10.cloned.1.call-update) | async-done | bytes 2162704 | tf_op jit(solution)/shard_map/all_gather | solution.py:30
  35.2 63.3 %all-gather.14.cloned.1.call-done = bf16[2112,704]{1,0:T(8,128)(2,1)} async-done(((bf16[264,704]{1,0:T(8,128)(2,1)}), bf16[2112,704]{1,0:T(8,128)(2,1)}) %all-gather.14.cloned.1.call-update) | async-done | bytes 2973712 | tf_op jit(solution)/shard_map/all_gather | solution.py:34
  98.5 4.5 %convolution_convert_fusion = bf16[512,704]{0,1:T(8,128)(2,1)S(1)} fusion(bf16[512,2112]{0,1:T(8,128)(2,1)} %all-gather.10.cloned.1.call-done, bf16[2112,704]{1,0:T(8,128)(2,1)} %all-gather.14.cloned.1.call-done), kind=kOutput, calls=%fused_computation.26 | convolution fusion | flops 1522892800 | bytes 5857280 | tf_op jit(solution)/shard_map/dot_general | solution.py:44
  103.1 2.5 collective-permute-start
  105.5 16.1 %all-gather.6.cloned.1.call-done = bf16[512,2112]{0,1:T(8,128)(2,1)} async-done(((bf16[512,528]{0,1:T(8,128)(2,1)}), bf16[512,2112]{0,1:T(8,128)(2,1)}) %all-gather.6.cloned.1.call-update) | async-done | bytes 2162704 | tf_op jit(solution)/shard_map/all_gather | solution.py:31
  121.7 63.1 %all-gather.8.cloned.1.call-done = bf16[704,2112]{0,1:T(8,128)(2,1)} async-done(((bf16[704,264]{0,1:T(8,128)(2,1)}), bf16[704,2112]{0,1:T(8,128)(2,1)}) %all-gather.8.cloned.1.call-update) | async-done | bytes 2973712 | tf_op jit(solution)/shard_map/all_gather | solution.py:40
  184.8 4.5 %convolution_convert_fusion.2 = bf16[512,704]{0,1:T(8,128)(2,1)S(1)} fusion(bf16[512,2112]{0,1:T(8,128)(2,1)} %all-gather.6.cloned.1.call-done, bf16[704,2112]{0,1:T(8,128)(2,1)} %all-gather.8.cloned.1.call-done), kind=kOutput, calls=%fused_computation.28 | convolution fusion | flops 1522892800 | bytes 5857280 | tf_op jit(solution)/shard_map/dot_general | solution.py:38
  189.7 2.4 add_add_fusion
  192.1 54.5 %all-gather.12.cloned.1.call-done = bf16[2112,704]{1,0:T(8,128)(2,1)} async-done(((bf16[264,704]{1,0:T(8,128)(2,1)}), bf16[2112,704]{1,0:T(8,128)(2,1)}) %all-gather.12.cloned.1.call-update) | async-done | bytes 2973712 | tf_op jit(solution)/shard_map/all_gather | solution.py:35
  246.6 5.3 %fusion.6 = f32[512,704]{0,1:T(8,128)S(1)} fusion(bf16[512,704]{0,1:T(8,128)(2,1)S(1)} %convolution_convert_fusion.2, f32[512,704]{0,1:T(8,128)} %add_add_fusion, bf16[512,2112]{0,1:T(8,128)(2,1)} %all-gather.10.cloned.1.call-done, bf16[2112,704]{1,0:T(8,128)(2,1)} %all-gather.12.cloned.1.call-done), kind=kOutput, calls=%fused_computation.13 | convolution fusion | flops 1527218176 | bytes 8740864 | tf_op jit(solution)/shard_map/dot_general | solution.py:45
  251.9 1.4 collective-permute-start.1
  253.4 9.0 %collective-permute-done.1 = f32[2,704]{0,1:T(8,128)S(1)} collective-permute-done((f32[2,704]{0,1:T(8,128)S(1)}, f32[2,704]{0,1:T(8,128)S(1)}, u32[]{:S(2)}, u32[]{:S(2)}) %collective-permute-start.1) | collective-permute-done | bytes 5664 | tf_op jit(solution)/shard_map/ppermute | solution.py:13
  262.3 3.2 multiply_reduce_fusion.2
  265.6 4.5 %convolution_bitcast_fusion = f32[2112,704]{0,1:T(8,128)} fusion(bf16[512,704]{0,1:T(8,128)(2,1)S(1)} %get-tuple-element.22, bf16[512,2112]{0,1:T(8,128)(2,1)S(1)} %copy-done), kind=kOutput, calls=%fused_computation | convolution fusion | flops 1522532352 | bytes 8830976 | tf_op jit(solution)/shard_map/dot_general | solution.py:72
  270.1 7.2 %copy.14 = f32[2112,704]{1,0:T(8,128)} copy(f32[2112,704]{0,1:T(8,128)} %convolution_bitcast_fusion) | data formatting | bytes 11894784
  277.5 3.9 fusion.14
  281.5 3.3 fusion
  285.2 44.6 %psum.15 = f32[4,2816]{1,0:T(4,128)S(1)} all-reduce(f32[4,2816]{1,0:T(4,128)S(1)} %dynamic_update_slice.3), channel_id=1, replica_groups=mesh['fs'=8,'tp'=4] {'fs','tp'}, use_global_device_ids=true, to_apply=%region_8.0 | all-reduce | flops 11264 | bytes 90112 | tf_op jit(solution)/shard_map/psum | solution.py:82
  330.5 70.1 %reduce-scatter.7.cloned.1.call-done = f32[264,704]{1,0:T(8,128)} async-done(((f32[2112,704]{1,0:T(8,128)}), f32[264,704]{1,0:T(8,128)}) %reduce-scatter.7.cloned.1.call-update) | async-done | bytes 743440
  400.6 1.5 copy.15
  402.3 20.3 %psum.14 = f32[704]{0:T(1024)} all-reduce(f32[704]{0:T(1024)S(1)} %multiply_reduce_fusion.3), channel_id=1, replica_groups=mesh['fs'=8,'tp'=4] {'fs'}, use_global_device_ids=true, to_apply=%region_3.0 | all-reduce | flops 704 | bytes 5632 | tf_op jit(solution)/shard_map/psum | solution.py:83
  422.6 12.0 %reduce-scatter.5.cloned.1.call-done = bf16[512,528]{0,1:T(8,128)(2,1)} async-done(((bf16[512,2112]{0,1:T(8,128)(2,1)}), bf16[512,528]{0,1:T(8,128)(2,1)}) %reduce-scatter.5.cloned.1.call-update) | async-done | bytes 540688 | tf_op jit(solution)/shard_map/reduce_scatter | solution.py:67
  (35 shorter events, 5.3 us)
Async XLA Ops:
  7.2 28.1 %all-gather.10.cloned.1.call-start = ((), (), s32[]{:S(2)}) async-start(), calls=%async_computation.4 | async-start | bytes 2703360 | tf_op jit(solution)/shard_map/all_gather | solution.py:30
  7.9 90.6 %all-gather.14.cloned.1.call-start = ((), (), s32[]{:S(2)}) async-start(), calls=%async_computation.6 | async-start | bytes 3649536 | tf_op jit(solution)/shard_map/all_gather | solution.py:34
  8.6 113.0 %all-gather.6.cloned.1.call-start = ((), (), s32[]{:S(2)}) async-start(), calls=%async_computation.2 | async-start | bytes 2703360 | tf_op jit(solution)/shard_map/all_gather | solution.py:31
  9.4 175.4 %all-gather.8.cloned.1.call-start = ((), (), s32[]{:S(2)}) async-start(), calls=%async_computation.3 | async-start | bytes 3649536 | tf_op jit(solution)/shard_map/all_gather | solution.py:40
  10.0 236.7 %all-gather.12.cloned.1.call-start = ((), (), s32[]{:S(2)}) async-start(), calls=%async_computation.5 | async-start | bytes 3649536 | tf_op jit(solution)/shard_map/all_gather | solution.py:35
  10.5 390.1 %reduce-scatter.7.cloned.1.call-start = ((), (), s32[]{:S(2)}) async-start(), calls=%async_computation.8 | async-start | bytes 7299072
  103.1 86.2 %collective-permute-start = (bf16[2,704]{0,1:T(8,128)(2,1)S(1)}, bf16[2,704]{0,1:T(8,128)(2,1)S(1)}, u32[]{:S(2)}, u32[]{:S(2)}) collective-permute-start(bf16[2,704]{0,1:T(8,128)(2,1)S(1)} %slice.54), channel_id=1, source_target_pairs={{0,4},{4,8},{8,12},{12,16},{16,20},{20,24},{24,28},{1,5},{5,9},{9,... | collective-permute-start | bytes 8456 | tf_op jit(solution)/shard_map/ppermute | solution.py:13
  251.9 13.6 %copy-start = (bf16[512,2112]{0,1:T(8,128)(2,1)S(1)}, bf16[512,2112]{0,1:T(8,128)(2,1)}, u32[]{:S(2)}) copy-start(bf16[512,2112]{0,1:T(8,128)(2,1)} %all-gather.10.cloned.1.call-done) | copy-start | bytes 6488068
  251.9 10.4 %collective-permute-start.1 = (f32[2,704]{0,1:T(8,128)S(1)}, f32[2,704]{0,1:T(8,128)S(1)}, u32[]{:S(2)}, u32[]{:S(2)}) collective-permute-start(f32[2,704]{0,1:T(8,128)S(1)} %slice.58), channel_id=1, source_target_pairs={{4,0},{8,4},{12,8},{16,12},{20,16},{24,20},{28,24},{5,1},{9,5},{13... | collective-permute-start | bytes 16904 | tf_op jit(solution)/shard_map/ppermute | solution.py:13
  277.3 4.2 copy-start.1
  277.3 157.3 %reduce-scatter.5.cloned.1.call-start = ((), (), s32[]{:S(2)}) async-start(), calls=%async_computation.7 | async-start | bytes 2703360 | tf_op jit(solution)/shard_map/reduce_scatter | solution.py:67
  277.5 3.9 copy-start.3
  329.9 72.4 %copy-start.2 = (f32[4,2816]{1,0:T(4,128)}, f32[4,2816]{1,0:T(4,128)S(1)}, u32[]{:S(2)}) copy-start(f32[4,2816]{1,0:T(4,128)S(1)} %psum.15) | copy-start | bytes 135172
Sparse Core Ops, SparseCore 0:
  9.5 25.6 all-gather.9
  37.4 61.0 all-gather.13
  100.1 21.5 all-gather.5
  123.7 61.0 all-gather.7
  186.8 59.7 all-gather.11
  277.4 123.1 reduce-scatter.6
  403.7 30.8 reduce-scatter.4
where the time goes:
time: 442 us; the launch traced here: 441 us
  waiting for transfers between devices  314 us (71%)
  blocking collectives  64.9 us (15%)
  matrix products  25.9 us (6%)
  between operations  14.3 us (3%)
  local copies, waits for them, and re-layouts  11.5 us (3%)
  other arithmetic  6.2 us (1%)
    unnamed x8, waiting for transfers between devices  73.2 us
    all_gather x1, waiting for transfers between devices, per_device(): lax.all_gather(w_conv_up, 'fs', axis=0, tiled=True)  63.3 us
    all_gather x1, waiting for transfers between devices, per_device(): lax.all_gather(w_down, 'fs', axis=1, tiled=True)  63.1 us
    all_gather x1, waiting for transfers between devices, per_device(): lax.all_gather(w_gate_up, 'fs', axis=0, tiled=True)  54.5 us
    psum x1, blocking collectives, per_device(): full_columns = lax.psum(placed, ('fs', 'tp'))  44.6 us
    all_gather x1, waiting for transfers between devices, per_device(): lax.all_gather(inputs, 'tp', axis=1, tiled=True)  22.9 us
    psum x1, blocking collectives, per_device(): unit_norms = lax.psum(squares, 'fs')  20.3 us
    all_gather x1, waiting for transfers between devices, per_device(): lax.all_gather(cotangent, 'tp', axis=1, tiled=True)  16.1 us
  transfers between devices with their start and end apart: 9, of which 8 were waited for; matrix products, arithmetic and copies ran while one was open for 5% of the time, Pallas kernels for 0%

commit v1 on v0

--- a/solution.py
+++ b/solution.py
@@ -5,6 +5,11 @@
 from jax.sharding import PartitionSpec as P
 
 TAPS = 3
+
+
+def gather_and_add(x, axis):
+    blocks = lax.all_gather(x, axis)
+    return jnp.sum(blocks, axis=0)
 
 
 def shifted(block, axis, distance):
@@ -79,7 +84,7 @@
     squares = jnp.sum(grad_conv_up * grad_conv_up, axis=0)
     placed = jnp.zeros((TAPS + 1, width * lax.axis_size("tp")), jnp.float32)
     placed = lax.dynamic_update_slice_in_dim(placed, column_part, col_start, 1)
-    full_columns = lax.psum(placed, ("fs", "tp"))
+    full_columns = gather_and_add(placed, ("fs", "tp"))
     unit_norms = lax.psum(squares, "fs")
     return (grad_inputs, grad_conv_up, unit_norms, full_columns[:TAPS], full_columns[TAPS])
 

time: 442 us -> 488 us (1.10)
  waiting for transfers between devices: 314 us -> 401 us
  blocking collectives: 64.9 us -> 20.2 us
    unnamed x8 -> x9, waiting for transfers between devices: 73.2 us -> 126 us
    psum x1 -> x0, blocking collectives: 44.6 us -> none  [per_device(): full_columns = lax.psum(placed, ('fs', 'tp'))]
    all_gather x0 -> x1, waiting for transfers between devices: none -> 34.3 us  [gather_and_add(): blocks = lax.all_gather(x, axis)]
  transfers between devices with their start and end apart: 9 -> 10, of which waited for: 8 -> 9; matrix products, arithmetic and copies ran while one was open for 5% -> 8% of each run, Pallas kernels for 0% -> 0%
where the time goes in v1:
time: 488 us; the launch traced here: 487 us
  waiting for transfers between devices  401 us (82%)
  matrix products  27.5 us (6%)
  blocking collectives  20.2 us (4%)
  between operations  14.3 us (3%)
  local copies, waits for them, and re-layouts  12.1 us (2%)
  other arithmetic  7.78 us (2%)
    unnamed x9, waiting for transfers between devices  126 us
    all_gather x1, waiting for transfers between devices, per_device(): lax.all_gather(w_conv_up, 'fs', axis=0, tiled=True)  63.3 us
    all_gather x1, waiting for transfers between devices, per_device(): lax.all_gather(w_down, 'fs', axis=1, tiled=True)  63.1 us
    all_gather x1, waiting for transfers between devices, per_device(): lax.all_gather(w_gate_up, 'fs', axis=0, tiled=True)  54.5 us
    all_gather x1, waiting for transfers between devices, gather_and_add(): blocks = lax.all_gather(x, axis)  34.3 us
    all_gather x1, waiting for transfers between devices, per_device(): lax.all_gather(inputs, 'tp', axis=1, tiled=True)  22.9 us
    psum x1, blocking collectives, per_device(): unit_norms = lax.psum(squares, 'fs')  20.2 us
    all_gather x1, waiting for transfers between devices, per_device(): lax.all_gather(cotangent, 'tp', axis=1, tiled=True)  16.1 us
  transfers between devices with their start and end apart: 10, of which 9 were waited for; matrix products, arithmetic and copies ran while one was open for 8% of the time, Pallas kernels for 0%

profile of v1, /device:TPU:0, one launch (start us, length us, event | category | flops | bytes accessed | tf_op | source)
XLA Modules:
  0.0 487.4 jit_solution(14230752323974878052)
XLA Ops:
  11.4 0.9 dynamic-slice_reduce_fusion.2
  12.3 22.9 %all-gather.11.cloned.1.call-done = bf16[512,2112]{0,1:T(8,128)(2,1)} async-done(((bf16[512,528]{0,1:T(8,128)(2,1)}), bf16[512,2112]{0,1:T(8,128)(2,1)}) %all-gather.11.cloned.1.call-update) | async-done | bytes 2162704 | tf_op jit(solution)/shard_map/all_gather | solution.py:35
  35.2 63.3 %all-gather.15.cloned.1.call-done = bf16[2112,704]{1,0:T(8,128)(2,1)} async-done(((bf16[264,704]{1,0:T(8,128)(2,1)}), bf16[2112,704]{1,0:T(8,128)(2,1)}) %all-gather.15.cloned.1.call-update) | async-done | bytes 2973712 | tf_op jit(solution)/shard_map/all_gather | solution.py:39
  98.5 4.5 convolution_convert_fusion
  103.1 2.5 collective-permute-start
  105.5 16.1 %all-gather.7.cloned.1.call-done = bf16[512,2112]{0,1:T(8,128)(2,1)} async-done(((bf16[512,528]{0,1:T(8,128)(2,1)}), bf16[512,2112]{0,1:T(8,128)(2,1)}) %all-gather.7.cloned.1.call-update) | async-done | bytes 2162704 | tf_op jit(solution)/shard_map/all_gather | solution.py:36
  121.7 63.1 %all-gather.9.cloned.1.call-done = bf16[704,2112]{0,1:T(8,128)(2,1)} async-done(((bf16[704,264]{0,1:T(8,128)(2,1)}), bf16[704,2112]{0,1:T(8,128)(2,1)}) %all-gather.9.cloned.1.call-update) | async-done | bytes 2973712 | tf_op jit(solution)/shard_map/all_gather | solution.py:45
  184.8 4.5 convolution_convert_fusion.2
  189.7 2.4 add_add_fusion
  192.1 54.5 %all-gather.13.cloned.1.call-done = bf16[2112,704]{1,0:T(8,128)(2,1)} async-done(((bf16[264,704]{1,0:T(8,128)(2,1)}), bf16[2112,704]{1,0:T(8,128)(2,1)}) %all-gather.13.cloned.1.call-update) | async-done | bytes 2973712 | tf_op jit(solution)/shard_map/all_gather | solution.py:40
  246.6 5.3 %fusion.6 = f32[512,704]{0,1:T(8,128)S(1)} fusion(bf16[512,704]{0,1:T(8,128)(2,1)S(1)} %convolution_convert_fusion.2, f32[512,704]{0,1:T(8,128)} %add_add_fusion, bf16[512,2112]{0,1:T(8,128)(2,1)} %all-gather.11.cloned.1.call-done, bf16[2112,704]{1,0:T(8,128)(2,1)} %all-gather.13.cloned.1.call-done), kind=kOutput, calls=%fused_computation.13 | convolution fusion | flops 1527218176 | bytes 8740864 | tf_op jit(solution)/shard_map/dot_general | solution.py:50
  251.9 1.3 collective-permute-start.1
  253.2 9.0 %collective-permute-done.1 = f32[2,704]{0,1:T(8,128)S(1)} collective-permute-done((f32[2,704]{0,1:T(8,128)S(1)}, f32[2,704]{0,1:T(8,128)S(1)}, u32[]{:S(2)}, u32[]{:S(2)}) %collective-permute-start.1) | collective-permute-done | bytes 5664 | tf_op jit(solution)/shard_map/ppermute | solution.py:18
  262.2 3.2 multiply_reduce_fusion.2
  266.5 6.1 %convolution_bitcast_fusion = f32[2112,704]{0,1:T(8,128)} fusion(bf16[512,704]{0,1:T(8,128)(2,1)S(1)} %get-tuple-element.22, bf16[512,2112]{0,1:T(8,128)(2,1)} %all-gather.11.cloned.1.call-done), kind=kOutput, calls=%fused_computation | convolution fusion | flops 1522532352 | bytes 8830976 | tf_op jit(solution)/shard_map/dot_general | solution.py:77
  272.6 7.2 %copy.14 = f32[2112,704]{1,0:T(8,128)} copy(f32[2112,704]{0,1:T(8,128)} %convolution_bitcast_fusion) | data formatting | bytes 11894784
  280.1 3.9 fusion.14
  284.0 3.3 fusion
  287.4 34.3 %all-gather.17.cloned.1.call-done = f32[32,4,2816]{2,1,0:T(4,128)} async-done(((f32[1,4,2816]{2,1,0:T(4,128)}), f32[32,4,2816]{2,1,0:T(4,128)}) %all-gather.17.cloned.1.call-update) | async-done | bytes 1441808 | tf_op jit(solution)/shard_map/all_gather | solution.py:11
  321.7 1.6 reduce_sum.59
  323.9 122.7 %reduce-scatter.7.cloned.1.call-done = f32[264,704]{1,0:T(8,128)} async-done(((f32[2112,704]{1,0:T(8,128)}), f32[264,704]{1,0:T(8,128)}) %reduce-scatter.7.cloned.1.call-update) | async-done | bytes 743440
  446.6 1.5 copy.15
  448.3 20.2 %psum.7 = f32[704]{0:T(1024)} all-reduce(f32[704]{0:T(1024)S(1)} %multiply_reduce_fusion.3), channel_id=1, replica_groups=mesh['fs'=8,'tp'=4] {'fs'}, use_global_device_ids=true, to_apply=%region_3.0 | all-reduce | flops 704 | bytes 5632 | tf_op jit(solution)/shard_map/psum | solution.py:88
  468.6 12.0 %reduce-scatter.5.cloned.1.call-done = bf16[512,528]{0,1:T(8,128)(2,1)} async-done(((bf16[512,2112]{0,1:T(8,128)(2,1)}), bf16[512,528]{0,1:T(8,128)(2,1)}) %reduce-scatter.5.cloned.1.call-update) | async-done | bytes 540688 | tf_op jit(solution)/shard_map/reduce_scatter | solution.py:72
  (38 shorter events, 6.8 us)
Async XLA Ops:
  7.2 28.1 %all-gather.11.cloned.1.call-start = ((), (), s32[]{:S(2)}) async-start(), calls=%async_computation.4 | async-start | bytes 2703360 | tf_op jit(solution)/shard_map/all_gather | solution.py:35
  7.9 90.6 %all-gather.15.cloned.1.call-start = ((), (), s32[]{:S(2)}) async-start(), calls=%async_computation.6 | async-start | bytes 3649536 | tf_op jit(solution)/shard_map/all_gather | solution.py:39
  8.6 113.0 %all-gather.7.cloned.1.call-start = ((), (), s32[]{:S(2)}) async-start(), calls=%async_computation.2 | async-start | bytes 2703360 | tf_op jit(solution)/shard_map/all_gather | solution.py:36
  9.4 175.4 %all-gather.9.cloned.1.call-start = ((), (), s32[]{:S(2)}) async-start(), calls=%async_computation.3 | async-start | bytes 3649536 | tf_op jit(solution)/shard_map/all_gather | solution.py:45
  10.0 236.7 %all-gather.13.cloned.1.call-start = ((), (), s32[]{:S(2)}) async-start(), calls=%async_computation.5 | async-start | bytes 3649536 | tf_op jit(solution)/shard_map/all_gather | solution.py:40
  10.5 311.1 %all-gather.17.cloned.1.call-start = ((), (), s32[]{:S(2)}) async-start(), calls=%async_computation.8 | async-start | bytes 1486848 | tf_op jit(solution)/shard_map/all_gather | solution.py:11
  103.1 86.2 %collective-permute-start = (bf16[2,704]{0,1:T(8,128)(2,1)S(1)}, bf16[2,704]{0,1:T(8,128)(2,1)S(1)}, u32[]{:S(2)}, u32[]{:S(2)}) collective-permute-start(bf16[2,704]{0,1:T(8,128)(2,1)S(1)} %slice.54), channel_id=1, source_target_pairs={{0,4},{4,8},{8,12},{12,16},{16,20},{20,24},{24,28},{1,5},{5,9},{9,... | collective-permute-start | bytes 8456 | tf_op jit(solution)/shard_map/ppermute | solution.py:18
  251.9 10.3 %collective-permute-start.1 = (f32[2,704]{0,1:T(8,128)S(1)}, f32[2,704]{0,1:T(8,128)S(1)}, u32[]{:S(2)}, u32[]{:S(2)}) collective-permute-start(f32[2,704]{0,1:T(8,128)S(1)} %slice.58), channel_id=1, source_target_pairs={{4,0},{8,4},{12,8},{16,12},{20,16},{24,20},{28,24},{5,1},{9,5},{13... | collective-permute-start | bytes 16904 | tf_op jit(solution)/shard_map/ppermute | solution.py:18
  265.8 0.6 copy-start.1
  266.5 180.1 %reduce-scatter.7.cloned.1.call-start = ((), (), s32[]{:S(2)}) async-start(), calls=%async_computation.9 | async-start | bytes 7299072
  279.9 4.2 copy-start
  279.9 200.7 %reduce-scatter.5.cloned.1.call-start = ((), (), s32[]{:S(2)}) async-start(), calls=%async_computation.7 | async-start | bytes 2703360 | tf_op jit(solution)/shard_map/reduce_scatter | solution.py:72
  280.1 3.9 copy-start.3
  323.2 125.1 %copy-start.2 = (f32[4,2816]{1,0:T(4,128)}, f32[4,2816]{1,0:T(4,128)S(1)}, u32[]{:S(2)}) copy-start(f32[4,2816]{1,0:T(4,128)S(1)} %reduce_sum.59) | copy-start | bytes 135172
Sparse Core Ops, SparseCore 0:
  9.5 25.6 all-gather.10
  37.4 61.0 all-gather.14
  100.1 21.5 all-gather.6
  123.7 61.0 all-gather.8
  186.8 59.7 all-gather.12
  266.6 55.0 all-gather.16
  325.8 120.7 reduce-scatter.6
  449.7 30.7 reduce-scatter.4
